TPU v7x, 512 devices: a whole 4x4x16 slice. The times are simulated.
512 devices in a mesh: sp: 32 (over z, core), tp: 16 (over y, x).
Axes of the slice: x: 4, y: 4, z: 16, core: 2. Of those that a mesh axis runs over, the one named last changes fastest.
Arguments:
- query_pre: bfloat16 [16384, 2048], P('sp', 'tp'), may hold values from -6 to 6
- forget_pre: bfloat16 [16384, 2048], P('sp', 'tp'), may hold values from -8 to 8
- values_in: bfloat16 [16384, 2048], P('sp', 'tp'), may hold values from -16 to 16
- gate_pre: bfloat16 [16384, 2048], P('sp', 'tp'), may hold values from -6 to 6
- floor_gap: float32 [2048], P('tp'), may hold values from 0 to 1, as said below
- head_gain: float32 [128], replicated, may hold values from 0.1 to 1.9
- stream: bfloat16 [16384, 2048], P('sp', 'tp'), may hold values from -40 to 40
- out_proj: bfloat16 [2048, 2048], P(None, 'tp'), may hold values from -0.125 to 0.125
- norm_gain: float32 [2048], P('tp'), may hold values from 0.1 to 1.9
- route_ids: int32 [16384, 2], P('sp'), may hold values from 0 to 31, all different within a row; in each aligned block of 512 rows (0 to 511, 512 to 1023, ...) at most 64 rows name the same one
- route_weights: float32 [16384, 2], P('sp'), may hold values from 0.1 to 1.5
- expert_gate: bfloat16 [32, 2048, 2048], P('sp', None, 'tp'), may hold values from -0.125 to 0.125
- expert_up: bfloat16 [32, 2048, 2048], P('sp', None, 'tp'), may hold values from -0.125 to 0.125
- expert_down: bfloat16 [32, 2048, 2048], P('sp', None, 'tp'), may hold values from -0.125 to 0.125
- shared_gate: bfloat16 [2048, 2048], P(None, 'tp'), may hold values from -0.125 to 0.125
- shared_up: bfloat16 [2048, 2048], P(None, 'tp'), may hold values from -0.125 to 0.125
- shared_down: bfloat16 [2048, 2048], P(None, 'tp'), may hold values from -0.125 to 0.125
Outputs:
- layer_out: bfloat16 [16384, 2048], P('sp', 'tp')
Inputs may be any that keep to these rules, and one draw needn't show every extreme that they name: `route_ids`: in each aligned block of 512 rows every expert is named by at most 64 rows, a bound that some block reaches; the 2 experts of a row differ. `floor_gap`: every entry is positive and at most 0.12.
All inputs are finite; a program needn't handle non-finite values.
Results may differ from a plain program's by a relative error of at most 0.008.
Values may be sent and summed in bfloat16 or wider, within the bound.
A program may use at most 64 MiB of HBM per device.

v0:
```python
import jax
import jax.numpy as jnp
from jax import lax
from jax.sharding import Mesh
from jax.sharding import PartitionSpec as P

D = 2048
HEAD = 128
SPAN = 64
TOP_K = 2
SP = ("sp_0", "sp_1")
TP = ("tp_0", "tp_1")
EPS = 1e-06


def neutral_like(value, identity):
    return jax.tree.map(
        lambda a, e: jnp.broadcast_to(jnp.asarray(e, a.dtype), a.shape), value, identity
    )


def gathered_once(value, axis):
    leaves = jax.tree.leaves(value)
    order = sorted(range(len(leaves)), key=lambda k: -leaves[k].size)
    width = (1, *leaves[order[0]].shape)[-1]
    lines = [
        jnp.pad(leaves[k].reshape(-1), (0, -leaves[k].size % width)).reshape(-1, width)
        for k in order
    ]
    both, at, found = (lax.all_gather(jnp.concatenate(lines), axis), 0, {})
    for k, line in zip(order, lines):
        slab = both[:, at : at + len(line)].reshape(len(both), -1)
        found[k] = slab[:, : leaves[k].size].reshape(-1, *leaves[k].shape)
        at += len(line)
    numbers = iter(range(len(leaves)))
    return jax.tree.map(lambda _: found[next(numbers)], value)


def prefix_by_axis(value, axes, combine, identity):
    before = start = neutral_like(value, identity)
    total = value
    for axis in reversed(axes):
        peers, mine = (lax.axis_size(axis), lax.axis_index(axis))
        pieces = gathered_once(total, axis)
        inside, total = (start, start)
        for k in range(peers):
            passed = k < mine
            total = combine(total, jax.tree.map(lambda part: part[k], pieces))
            inside = jax.tree.map(lambda new, old: jnp.where(passed, new, old), total, inside)
        before = combine(inside, before)
    return before


def sent_to_all(value, axis):
    copies = jnp.broadcast_to(value, (lax.axis_size(axis), *value.shape))
    return lax.all_to_all(copies, axis, split_axis=0, concat_axis=0, tiled=True)


def joined_along(pieces, dim):
    lengths = list(pieces.shape[1:])
    lengths[dim] *= pieces.shape[0]
    return jnp.moveaxis(pieces, 0, dim).reshape(lengths)


def gather_directly(value, axis, dim):
    pieces = sent_to_all(value, axis)
    return joined_along(pieces, dim)


def one_axis_at_a_time(value, axes):
    for axis in axes:
        value = lax.psum(value, axis)
    return value


def sent_together(arrays, axis, dim, along):
    widths = [a.shape[along] for a in arrays]
    both = jnp.concatenate(arrays, axis=along)
    filled = lax.all_gather(both, axis, axis=dim, tiled=True)
    return tuple(jnp.split(filled, [sum(widths[:k]) for k in range(1, len(widths))], axis=along))


def span_step(memory, blocks):
    queries, leakage, values, log_keep = blocks
    length = queries.shape[1]
    growth = jnp.cumsum(log_keep, axis=1)
    causal = jnp.tril(jnp.ones((length, length), dtype=bool))
    spread = growth[:, :, None, :] - growth[:, None, :, :]
    decays = jnp.exp(jnp.where(causal[None, :, :, None], spread, -jnp.inf))
    scores = jnp.einsum("htd,hsd,htsd->hts", queries, leakage, decays)
    within = jnp.einsum("hts,hsv->htv", scores, values)
    carried = jnp.einsum("htd,hdv->htv", queries * jnp.exp(growth), memory)
    closing = growth[:, -1:, :]
    memory = jnp.exp(closing[:, 0, :, None]) * memory + jnp.einsum(
        "hsd,hsv->hdv", leakage * jnp.exp(closing - growth), values
    )
    return (memory, within + carried)


def recurrence(queries, leakage, values, log_keep, memory):
    head_count, length, channels = queries.shape
    number = length // SPAN

    def blocked(array):
        return array.reshape(head_count, number, SPAN, channels).transpose(1, 0, 2, 3)

    memory, outputs = lax.scan(
        span_step, memory, (blocked(queries), blocked(leakage), blocked(values), blocked(log_keep))
    )
    return outputs.transpose(1, 0, 2, 3).reshape(head_count, length, channels)


def chain(earlier, later):
    return (earlier[0] * later[0], later[0][:, :, None] * earlier[1] + later[1])


def pad_rows(array):
    return jnp.concatenate([array, jnp.zeros((1, array.shape[1]), array.dtype)], axis=0)


def matmul(left, right):
    return jnp.dot(left, right, preferred_element_type=jnp.float32)


def body(
    query_pre,
    forget_pre,
    values_in,
    gate_pre,
    floor_gap,
    head_gain,
    stream,
    out_proj,
    norm_gain,
    route_ids,
    route_weights,
    expert_gate,
    expert_up,
    expert_down,
    shared_gate,
    shared_up,
    shared_down,
):
    length, local = query_pre.shape
    head_count = local // HEAD

    def split_heads(array):
        return array.astype(jnp.float32).reshape(length, head_count, HEAD).transpose(1, 0, 2)

    queries = jax.nn.silu(split_heads(query_pre))
    leakage = floor_gap.reshape(head_count, 1, HEAD) * jax.nn.sigmoid(-split_heads(forget_pre))
    log_keep = jnp.log1p(-leakage)
    values = split_heads(values_in)
    growth = jnp.cumsum(log_keep, axis=1)
    closing = growth[:, -1:, :]
    summary = jnp.einsum("hsd,hsv->hdv", leakage * jnp.exp(closing - growth), values)
    through = jnp.exp(closing[:, 0, :])
    unused, incoming = prefix_by_axis(
        (through, summary), SP, chain, (jnp.ones_like(through), jnp.zeros_like(summary))
    )
    outputs = recurrence(queries, leakage, values, log_keep, jnp.zeros_like(summary))
    outputs = outputs + jnp.einsum("htd,hdv->htv", queries * jnp.exp(growth), incoming)
    scaled = (
        outputs * lax.rsqrt(jnp.mean(outputs * outputs, axis=2, keepdims=True) + EPS) * head_gain
    )
    gated = scaled * jax.nn.silu(split_heads(gate_pre))
    mixed = gated.transpose(1, 0, 2).reshape(length, local).astype(jnp.bfloat16)
    projected = matmul(gather_directly(mixed, TP, 1), out_proj)
    residual = stream.astype(jnp.float32) + projected
    squares = one_axis_at_a_time(jnp.sum(residual * residual, axis=1), TP)
    normed = (residual * lax.rsqrt(squares / D + EPS)[:, None] * norm_gain).astype(jnp.bfloat16)
    experts = lax.axis_size(SP) * expert_gate.shape[0]
    capacity = 2 * TOP_K * length // experts
    flat_ids = route_ids.reshape(-1)
    matches = (flat_ids[:, None] == jnp.arange(experts, dtype=jnp.int32)[None, :]).astype(jnp.int32)
    earlier_hits = jnp.cumsum(matches, axis=0) - matches
    target = flat_ids * capacity + jnp.sum(earlier_hits * matches, axis=1)
    sender = (
        jnp.full((experts * capacity,), length, jnp.int32)
        .at[target]
        .set(jnp.arange(length * TOP_K, dtype=jnp.int32) // TOP_K)
    )
    gate_slice = expert_gate[0]
    up_slice = expert_up[0]
    down_slice = expert_down[0]
    arrived = lax.all_to_all(pad_rows(normed)[sender], SP, split_axis=0, concat_axis=0, tiled=True)
    own_rows, routed_rows = sent_together((normed, arrived), TP, 1, 0)
    shared_gate_part = matmul(own_rows, shared_gate)
    shared_up_part = matmul(own_rows, shared_up)
    routed_gate_part = matmul(routed_rows, gate_slice)
    routed_up_part = matmul(routed_rows, up_slice)
    shared_hidden = (jax.nn.silu(shared_gate_part) * shared_up_part).astype(jnp.bfloat16)
    routed_hidden = (jax.nn.silu(routed_gate_part) * routed_up_part).astype(jnp.bfloat16)
    full_shared, full_routed = (
        lax.all_gather(shared_hidden, TP, axis=1, tiled=True),
        lax.all_gather(routed_hidden, TP, axis=1, tiled=True),
    )
    shared_out = matmul(full_shared, shared_down)
    expert_result = matmul(full_routed, down_slice).astype(jnp.bfloat16)
    returned = lax.all_to_all(expert_result, SP, split_axis=0, concat_axis=0, tiled=True)
    picked = returned[target].astype(jnp.float32).reshape(length, TOP_K, returned.shape[1])
    routed = jnp.sum(picked * route_weights[:, :, None], axis=1)
    return (residual + shared_out + routed).astype(jnp.bfloat16)


def solution(mesh):
    finer = Mesh(mesh.devices.reshape(16, 2, 4, 4), ("sp_0", "sp_1", "tp_0", "tp_1"))
    in_specs = (
        P(SP, TP),
        P(SP, TP),
        P(SP, TP),
        P(SP, TP),
        P(TP),
        P(),
        P(SP, TP),
        P(None, TP),
        P(TP),
        P(SP, None),
        P(SP, None),
        P(SP, None, TP),
        P(SP, None, TP),
        P(SP, None, TP),
        P(None, TP),
        P(None, TP),
        P(None, TP),
    )
    out_specs = P(SP, TP)
    return jax.shard_map(body, mesh=finer, in_specs=in_specs, out_specs=out_specs, check_vma=False)
```

profile of v0, /device:TPU:2, one launch (start us, length us, event | category | flops | bytes accessed | tf_op | source)
XLA Modules:
  0.0 454.3 jit_solution(16247520927167944288)
XLA Ops:
  6.5 1.1 copy.79
  7.6 0.8 fusion.156
  10.2 1.9 all-gather.2
  12.2 0.6 maximum_bitcast_fusion.1
  13.5 24.4 %while.13 = (s32[]{:T(128)}, f32[1,128,128]{2,1,0:T(8,128)S(1)}, f32[8,1,64,128]{3,2,1,0:T(8,128)S(1)}, f32[8,1,64,128]{3,2,1,0:T(8,128)S(1)}, f32[8,1,64,128]{3...) while((s32[]{:T(128)}, f32[1,128,128]{2,1,0:T(8,128)S(1)}, ...), condition=%wide.region_2.3_spmd.clone, body=%wide.region_0.0_spmd.clone.sunk | while | flops 8478723 | bytes 5051520 | solution.py:107
  13.6 0.6 select_exponential_fusion.2
  14.3 1.7 fusion.187
  16.7 0.6 select_exponential_fusion.2
  17.3 1.7 fusion.187
  19.7 0.6 select_exponential_fusion.2
  20.4 1.7 fusion.187
  22.8 0.6 select_exponential_fusion.2
  23.4 1.7 fusion.187
  25.8 0.6 select_exponential_fusion.2
  26.5 1.7 fusion.187
  28.9 0.6 select_exponential_fusion.2
  29.5 1.7 fusion.187
  31.9 0.6 select_exponential_fusion.2
  32.6 1.7 fusion.187
  35.0 0.6 select_exponential_fusion.2
  35.6 1.7 fusion.187
  38.2 50.0 %all-gather.15.cloned.1.call-done = f32[16,129,128]{2,1,0:T(8,128)} async-done(((f32[1,129,128]{2,1,0:T(8,128)}), f32[16,129,128]{2,1,0:T(8,128)}) %all-gather.15.cloned.1.call-update) | async-done | bytes 1056784 | tf_op jit(solution)/shard_map/all_gather | solution.py:30
  88.2 0.8 slice_bitcast_fusion.17
  89.0 1.9 multiply_reduce_fusion.1
  91.0 1.6 broadcast_in_dim.48
  92.6 7.4 %all-to-all-start = ((bf16[16,512,128]{1,2,0:T(8,128)(2,1)}), bf16[16,512,128]{1,2,0:T(8,128)(2,1)S(1)}, u32[]{:S(2)}, u32[]{:S(2)}) async-start(bf16[16,512,128]{1,2,0:T(8,128)(2,1)} %broadcast_in_dim.48), calls=%async_computation | async-start | bytes 4194304 | tf_op jit(solution)/shard_map/all_to_all | solution.py:56
  100.6 9.0 %reduce-window.16 = s32[32,8,128]{2,1,0:T(8,128)S(1)} reduce-window(s32[32,8,128]{2,1,0:T(8,128)S(1)} %fusion.72, s32[]{:T(128)} %constant.41.clone.1), window={size=1x1x128 pad=0_0x0_0x127_0}, to_apply=%region_9.10 | reduce-window | flops 4161536 | bytes 262148 | tf_op jit(solution)/shard_map/reduce-window.2
  110.5 4.3 scatter_custom_fusion
  114.8 3.6 all-to-all-done
  118.4 1.9 multiply_reduce_fusion
  120.3 11.1 %psum.14 = f32[512]{0:T(512)S(1)} all-reduce(f32[512]{0:T(512)S(1)} %get-tuple-element.138), channel_id=1, replica_groups=mesh['sp_0'=16,'sp_1'=2,'tp_0'=4,'tp_1'=4] {'tp_0'}, use_global_device_ids=true, to_apply=%region_7.8 | all-reduce | flops 512 | bytes 4096 | tf_op jit(solution)/shard_map/psum | solution.py:72
  131.4 9.5 %psum.15 = f32[512]{0:T(512)S(1)} all-reduce(f32[512]{0:T(512)S(1)} %psum.14), channel_id=1, replica_groups=mesh['sp_0'=16,'sp_1'=2,'tp_0'=4,'tp_1'=4] {'tp_1'}, use_global_device_ids=true, to_apply=%region_8.9 | all-reduce | flops 512 | bytes 4096 | tf_op jit(solution)/shard_map/psum | solution.py:72
  141.1 6.2 %gather_fusion = bf16[2048,128]{1,0:T(8,128)(2,1)S(1)} fusion(bf16[513,128]{1,0:T(8,128)(2,1)S(1)} %concatenate.14, s32[2048]{0:T(1024)S(1)} %fusion.147), kind=kCustom, calls=%fused_computation | custom fusion | bytes 1056768 | tf_op jit(solution)/shard_map/gather | solution.py:186
  147.3 41.7 %all_to_all.29 = bf16[32,64,128]{2,1,0:T(8,128)(2,1)S(1)} all-to-all(bf16[32,64,128]{2,1,0:T(8,128)(2,1)S(1)} %bitcast.243), channel_id=1, replica_groups=mesh['sp_0'=16,'sp_1'=2,'tp_0'=4,'tp_1'=4] {'sp_0','sp_1'}, dimensions={0} | all-to-all | bytes 1048576 | tf_op jit(solution)/shard_map/all_to_all | solution.py:186
  189.0 0.9 pad_maximum_fusion
  190.1 90.3 %all-gather.9.cloned.1.call-done = bf16[2560,2048]{1,0:T(8,128)(2,1)} async-done(((bf16[2560,128]{1,0:T(8,128)(2,1)}), bf16[2560,2048]{1,0:T(8,128)(2,1)}) %all-gather.9.cloned.1.call-update) | async-done | bytes 10485776 | tf_op jit(solution)/shard_map/all_gather | solution.py:79
  280.4 5.9 %fusion.30 = f32[2048,128]{1,0:T(8,128)S(1)} fusion(bf16[2560,2048]{1,0:T(8,128)(2,1)} %all-gather.9.cloned.1.call-done, bf16[1,2048,128]{2,1,0:T(8,128)(2,1)S(1)} %copy-done), kind=kOutput, calls=%fused_computation.42 | convolution fusion | flops 1073741824 | bytes 9961472 | tf_op jit(solution)/shard_map/dot_general | solution.py:122
  286.8 3.2 fusion.35
  290.1 2.5 fusion.40
  292.6 3.1 fusion.47
  295.8 86.4 %all-gather.13.cloned.1.call-done = bf16[2048,2048]{1,0:T(8,128)(2,1)} async-done(((bf16[2048,128]{1,0:T(8,128)(2,1)}), bf16[2048,2048]{1,0:T(8,128)(2,1)}) %all-gather.13.cloned.1.call-update) | async-done | bytes 8388624 | tf_op jit(solution)/shard_map/all_gather | solution.py:196
  382.2 6.5 %convolution_convert_fusion = bf16[2048,128]{1,0:T(8,128)(2,1)} fusion(bf16[2048,2048]{1,0:T(8,128)(2,1)} %all-gather.13.cloned.1.call-done, bf16[1,2048,128]{2,1,0:T(8,128)(2,1)S(1)} %copy-done.15), kind=kOutput, calls=%fused_computation.45 | convolution fusion | flops 1074003968 | bytes 9437184 | tf_op jit(solution)/shard_map/dot_general | solution.py:122
  388.7 12.7 %all-to-all-start.2 = ((bf16[32,64,128]{2,1,0:T(8,128)(2,1)}), bf16[32,64,128]{2,1,0:T(8,128)(2,1)S(1)}, u32[]{:S(2)}, u32[]{:S(2)}) async-start(bf16[32,64,128]{2,1,0:T(8,128)(2,1)} %bitcast.52), calls=%async_computation.2 | async-start | bytes 1048576 | tf_op jit(solution)/shard_map/all_to_all | solution.py:200
  401.6 33.6 %all-to-all-done.2 = bf16[32,64,128]{2,1,0:T(8,128)(2,1)S(1)} async-done(((bf16[32,64,128]{2,1,0:T(8,128)(2,1)}), bf16[32,64,128]{2,1,0:T(8,128)(2,1)S(1)}, u32[]{:S(2)}, u32[]{:S(2)}) %all-to-all-start.2) | async-done | bytes 524320 | tf_op jit(solution)/shard_map/all_to_all | solution.py:200
  435.2 3.2 gather_fusion.1
  438.4 2.8 fusion.50
  441.2 3.5 all-gather.11.cloned.1.call-done
  444.8 3.0 fusion.46
  (163 shorter events, 10.4 us)
Async XLA Ops:
  6.5 273.9 %copy-start = (bf16[1,2048,128]{2,1,0:T(8,128)(2,1)S(1)}, bf16[1,2048,128]{2,1,0:T(8,128)(2,1)}, u32[]{:S(2)}) copy-start(bf16[1,2048,128]{2,1,0:T(8,128)(2,1)} %param.30) | copy-start | bytes 1572868
  6.5 81.7 %all-gather.15.cloned.1.call-start = ((), (), s32[]{:S(2)}) async-start(), calls=%async_computation.6 | async-start | bytes 1183744 | tf_op jit(solution)/shard_map/all_gather | solution.py:30
  8.4 1.4 copy-start.2
  8.5 1.4 copy-start.8
  9.6 3.5 copy-start.4
  13.5 24.6 %copy-start.5 = (bf16[512,128]{1,0:T(8,128)(2,1)S(1)}, bf16[512,128]{1,0:T(8,128)(2,1)}, u32[]{:S(2)}) copy-start(bf16[512,128]{1,0:T(8,128)(2,1)} %param.22) | copy-start | bytes 393220
  37.9 53.0 %copy-start.9 = (f32[128]{0:T(128)S(1)}, f32[128]{0:T(128)}, u32[]{:S(2)}) copy-start(f32[128]{0:T(128)} %param.24) | copy-start | bytes 1540
  92.6 7.5 %copy-start.6 = (s32[512,2]{0,1:T(2,128)S(1)}, s32[512,2]{0,1:T(2,128)}, u32[]{:S(2)}) copy-start(s32[512,2]{0,1:T(2,128)} %param.28) | copy-start | bytes 12292
  92.6 25.8 %all-to-all-start = ((bf16[16,512,128]{1,2,0:T(8,128)(2,1)}), bf16[16,512,128]{1,2,0:T(8,128)(2,1)S(1)}, u32[]{:S(2)}, u32[]{:S(2)}) async-start(bf16[16,512,128]{1,2,0:T(8,128)(2,1)} %broadcast_in_dim.48), calls=%async_computation | async-start | bytes 4194304 | tf_op jit(solution)/shard_map/all_to_all | solution.py:56
  100.0 18.4 %copy-start.3 = (bf16[512,128]{1,0:T(8,128)(2,1)S(1)}, bf16[512,128]{1,0:T(8,128)(2,1)}, u32[]{:S(2)}) copy-start(bf16[512,128]{1,0:T(8,128)(2,1)} %param.25) | copy-start | bytes 393220
  100.0 180.4 %all-gather.9.cloned.1.call-start = ((), (), s32[]{:S(2)}) async-start(), calls=%async_computation.3 | async-start | bytes 11141120 | tf_op jit(solution)/shard_map/all_gather | solution.py:79
  109.7 31.2 %copy-start.10 = (f32[128]{0:T(128)S(1)}, f32[128]{0:T(128)}, u32[]{:S(2)}) copy-start(f32[128]{0:T(128)} %param.27) | copy-start | bytes 1540
  189.9 96.5 %copy-start.12 = (bf16[1,2048,128]{2,1,0:T(8,128)(2,1)S(1)}, bf16[1,2048,128]{2,1,0:T(8,128)(2,1)}, u32[]{:S(2)}) copy-start(bf16[1,2048,128]{2,1,0:T(8,128)(2,1)} %param.31) | copy-start | bytes 1572868
  189.9 192.3 %all-gather.13.cloned.1.call-start = ((), (), s32[]{:S(2)}) async-start(), calls=%async_computation.5 | async-start | bytes 8912896 | tf_op jit(solution)/shard_map/all_gather | solution.py:196
  280.4 6.4 %copy-start.11 = (bf16[2560,2048]{1,0:T(8,128)(2,1)S(1)}, bf16[2560,2048]{1,0:T(8,128)(2,1)}, u32[]{:S(2)}) copy-start(bf16[2560,2048]{1,0:T(8,128)(2,1)} %all-gather.9.cloned.1.call-done) | copy-start | bytes 31457284
  286.8 3.3 copy-start.13
  290.0 2.6 copy-start.14
  290.1 154.7 %all-gather.11.cloned.1.call-start = ((), (), s32[]{:S(2)}) async-start(), calls=%async_computation.4 | async-start | bytes 2228224 | tf_op jit(solution)/shard_map/all_gather | solution.py:195
  292.6 89.6 %copy-start.15 = (bf16[1,2048,128]{2,1,0:T(8,128)(2,1)S(1)}, bf16[1,2048,128]{2,1,0:T(8,128)(2,1)}, u32[]{:S(2)}) copy-start(bf16[1,2048,128]{2,1,0:T(8,128)(2,1)} %param.32) | copy-start | bytes 1572868
  295.8 105.7 %copy-start.7 = (f32[512,2]{0,1:T(2,128)S(1)}, f32[512,2]{0,1:T(2,128)}, u32[]{:S(2)}) copy-start(f32[512,2]{0,1:T(2,128)} %param.29) | copy-start | bytes 12292
  388.7 56.0 %copy-start.1 = (bf16[2048,128]{1,0:T(8,128)(2,1)S(1)}, bf16[2048,128]{1,0:T(8,128)(2,1)}, u32[]{:S(2)}) copy-start(bf16[2048,128]{1,0:T(8,128)(2,1)} %param.35) | copy-start | bytes 1572868
  388.7 46.5 %all-to-all-start.2 = ((bf16[32,64,128]{2,1,0:T(8,128)(2,1)}), bf16[32,64,128]{2,1,0:T(8,128)(2,1)S(1)}, u32[]{:S(2)}, u32[]{:S(2)}) async-start(bf16[32,64,128]{2,1,0:T(8,128)(2,1)} %bitcast.52), calls=%async_computation.2 | async-start | bytes 1048576 | tf_op jit(solution)/shard_map/all_to_all | solution.py:200
Sparse Core Ops, SparseCore 0:
  13.0 75.1 all-gather.14
  190.0 90.3 all-gather.8
  290.2 91.9 all-gather.12
  385.1 59.6 all-gather.10
where the time goes:
time: 455 us; the launch traced here: 454 us
  waiting for transfers between devices  268 us (59%)
  blocking collectives  64.2 us (14%)
  other arithmetic  35.4 us (8%)
  matrix products  32.5 us (7%)
  starting transfers between devices  20.4 us (4%)
  local copies, waits for them, and re-layouts  20.2 us (4%)
  between operations  13.7 us (3%)
    all_gather x1, waiting for transfers between devices, sent_together(): filled = lax.all_gather(both, axis, axis=dim, tiled=True)  90.3 us
    all_gather x1, waiting for transfers between devices, body(): lax.all_gather(routed_hidden, TP, axis=1, tiled=True)  86.4 us
    all_gather x1, waiting for transfers between devices, gathered_once(): both, at, found = (lax.all_gather(jnp.concatenate(lines), axis), 0, {})  50 us
    all_to_all x1, blocking collectives, body(): lax.all_to_all(pad_rows(normed)[sender], SP, split_axis=0, concat_axis=0,...  41.7 us
    all_to_all x1, waiting for transfers between devices, body(): lax.all_to_all(expert_result, SP, split_axis=0, concat_axis=0, tiled=True)  33.6 us
    dot_general x7, matrix products, matmul(): return jnp.dot(left, right, preferred_element_type=jnp.float32)  26.2 us
    psum x2, blocking collectives, one_axis_at_a_time(): value = lax.psum(value, axis)  20.6 us
    dot_general x8, other arithmetic, span_step(): scores = jnp.einsum('htd,hsd,htsd->hts', queries, leakage, decays)  13.8 us
  transfers between devices with their start and end apart: 6, of which 6 were waited for; matrix products, arithmetic and copies ran while one was open for 13% of the time, Pallas kernels for 0%

commit v1 on v0

--- a/solution.py
+++ b/solution.py
@@ -193,7 +193,9 @@
     routed_hidden = (jax.nn.silu(routed_gate_part) * routed_up_part).astype(jnp.bfloat16)
     full_shared, full_routed = (
         lax.all_gather(shared_hidden, TP, axis=1, tiled=True),
-        lax.all_gather(routed_hidden, TP, axis=1, tiled=True),
+        jnp.concatenate(
+            lax.all_to_all(jnp.stack([routed_hidden] * lax.axis_size(TP)), TP, 0, 0), axis=1
+        ),
     )
     shared_out = matmul(full_shared, shared_down)
     expert_result = matmul(full_routed, down_slice).astype(jnp.bfloat16)

time: 455 us -> 501 us (1.10)
  the two profiles are of different devices: /device:TPU:2 before, /device:TPU:1 now
where the time goes in v1:
time: 501 us
  waiting for transfers between devices  283 us (56%)
  blocking collectives  77.6 us (15%)
  other arithmetic  38 us (8%)
  starting transfers between devices  30.8 us (6%)
  matrix products  30.6 us (6%)
  local copies, waits for them, and re-layouts  26.3 us (5%)
  between operations  13.7 us (3%)
    all_to_all x1, waiting for transfers between devices, body(): lax.all_to_all(jnp.stack([routed_hidden] * lax.axis_size(TP)), TP, 0, 0)  122 us
    all_gather x1, waiting for transfers between devices, sent_together(): filled = lax.all_gather(both, axis, axis=dim, tiled=True)  89.2 us
    all_to_all x1, blocking collectives, body(): lax.all_to_all(pad_rows(normed)[sender], SP, split_axis=0, concat_axis=0,...  54.8 us
    all_gather x1, waiting for transfers between devices, gathered_once(): both, at, found = (lax.all_gather(jnp.concatenate(lines), axis), 0, {})  33.6 us
    all_to_all x1, waiting for transfers between devices, body(): lax.all_to_all(expert_result, SP, split_axis=0, concat_axis=0, tiled=True)  33.3 us
    dot_general x7, matrix products, matmul(): return jnp.dot(left, right, preferred_element_type=jnp.float32)  24.3 us
    all_to_all x1, starting transfers between devices, body(): lax.all_to_all(expert_result, SP, split_axis=0, concat_axis=0, tiled=True)  18.8 us
    psum x2, blocking collectives, one_axis_at_a_time(): value = lax.psum(value, axis)  14.4 us
  transfers between devices with their start and end apart: 6, of which 5 were waited for; matrix products, arithmetic and copies ran while one was open for 12% of the time, Pallas kernels for 0%

profile of v1, /device:TPU:1, one launch (start us, length us, event | category | flops | bytes accessed | tf_op | source)
XLA Modules:
  0.0 500.7 jit_solution(8711588817396343911)
XLA Ops:
  6.5 1.1 copy.81
  7.6 0.8 fusion.156
  10.2 8.4 %all-gather.2 = f32[2,129,128]{2,1,0:T(8,128)S(1)} all-gather(f32[1,129,128]{2,1,0:T(8,128)S(1)} %maximum_bitcast_fusion), channel_id=2, replica_groups=mesh['sp_0'=16,'sp_1'=2,'tp_0'=4,'tp_1'=4] {'sp_1'}, dimensions={0}, use_global_device_ids=true | all-gather | bytes 198144 | tf_op jit(solution)/shard_map/all_gather | solution.py:30
  18.7 0.6 maximum_bitcast_fusion.1
  20.0 24.4 %while.13 = (s32[]{:T(128)}, f32[1,128,128]{2,1,0:T(8,128)S(1)}, f32[8,1,64,128]{3,2,1,0:T(8,128)S(1)}, f32[8,1,64,128]{3,2,1,0:T(8,128)S(1)}, f32[8,1,64,128]{3...) while((s32[]{:T(128)}, f32[1,128,128]{2,1,0:T(8,128)S(1)}, ...), condition=%wide.region_2.3_spmd.clone, body=%wide.region_0.0_spmd.clone.sunk | while | flops 8478723 | bytes 5052550 | solution.py:107
  20.2 0.6 select_exponential_fusion.2
  20.8 1.7 fusion.187
  23.8 1.7 fusion.187
  26.9 1.7 fusion.187
  30.0 1.7 fusion.187
  33.0 1.7 fusion.187
  36.1 1.7 fusion.187
  38.5 0.6 select_exponential_fusion.2
  39.1 1.7 fusion.187
  42.2 1.7 fusion.187
  44.8 33.6 %all-gather.12.cloned.1.call-done = f32[16,129,128]{2,1,0:T(8,128)} async-done(((f32[1,129,128]{2,1,0:T(8,128)}), f32[16,129,128]{2,1,0:T(8,128)}) %all-gather.12.cloned.1.call-update) | async-done | bytes 1056784 | tf_op jit(solution)/shard_map/all_gather | solution.py:30
  78.4 0.8 slice_bitcast_fusion.17
  79.1 1.9 multiply_reduce_fusion.1
  81.2 1.6 broadcast_in_dim.48
  82.8 7.1 %all-to-all-start = ((bf16[16,512,128]{1,2,0:T(8,128)(2,1)}), bf16[16,512,128]{1,2,0:T(8,128)(2,1)S(1)}, u32[]{:S(2)}, u32[]{:S(2)}) async-start(bf16[16,512,128]{1,2,0:T(8,128)(2,1)} %broadcast_in_dim.48), calls=%async_computation | async-start | bytes 4194304 | tf_op jit(solution)/shard_map/all_to_all | solution.py:56
  90.3 0.8 eq.25
  91.2 0.8 mul.467
  92.0 9.0 %reduce-window.16 = s32[32,8,128]{2,1,0:T(8,128)S(1)} reduce-window(s32[32,8,128]{2,1,0:T(8,128)S(1)} %fusion.72, s32[]{:T(128)} %constant.41.clone.1), window={size=1x1x128 pad=0_0x0_0x127_0}, to_apply=%region_9.10 | reduce-window | flops 4161536 | bytes 262148 | tf_op jit(solution)/shard_map/reduce-window.2
  102.0 0.7 fusion.70
  102.8 0.7 compare_select_fusion
  103.5 4.5 scatter_custom_fusion
  108.0 4.6 all-to-all-done
  112.6 0.8 multiply_reduce_fusion
  113.4 7.5 %psum.14 = f32[512]{0:T(512)S(1)} all-reduce(f32[512]{0:T(512)S(1)} %get-tuple-element.138), channel_id=1, replica_groups=mesh['sp_0'=16,'sp_1'=2,'tp_0'=4,'tp_1'=4] {'tp_0'}, use_global_device_ids=true, to_apply=%region_7.8 | all-reduce | flops 512 | bytes 4096 | tf_op jit(solution)/shard_map/psum | solution.py:72
  120.9 6.9 %psum.15 = f32[512]{0:T(512)S(1)} all-reduce(f32[512]{0:T(512)S(1)} %psum.14), channel_id=1, replica_groups=mesh['sp_0'=16,'sp_1'=2,'tp_0'=4,'tp_1'=4] {'tp_1'}, use_global_device_ids=true, to_apply=%region_8.9 | all-reduce | flops 512 | bytes 4096 | tf_op jit(solution)/shard_map/psum | solution.py:72
  127.9 0.8 multiply_convert_fusion
  128.7 6.2 %gather_fusion = bf16[2048,128]{1,0:T(8,128)(2,1)S(1)} fusion(bf16[513,128]{1,0:T(8,128)(2,1)S(1)} %concatenate.14, s32[2048]{0:T(1024)S(1)} %fusion.147), kind=kCustom, calls=%fused_computation | custom fusion | bytes 1056768 | tf_op jit(solution)/shard_map/gather | solution.py:186
  134.9 54.8 %all_to_all.34 = bf16[32,64,128]{2,1,0:T(8,128)(2,1)S(1)} all-to-all(bf16[32,64,128]{2,1,0:T(8,128)(2,1)S(1)} %bitcast.247), channel_id=1, replica_groups=mesh['sp_0'=16,'sp_1'=2,'tp_0'=4,'tp_1'=4] {'sp_0','sp_1'}, dimensions={0} | all-to-all | bytes 1048576 | tf_op jit(solution)/shard_map/all_to_all | solution.py:186
  189.6 0.9 pad_maximum_fusion
  190.6 89.2 %all-gather.8.cloned.1.call-done = bf16[2560,2048]{1,0:T(8,128)(2,1)} async-done(((bf16[2560,128]{1,0:T(8,128)(2,1)}), bf16[2560,2048]{1,0:T(8,128)(2,1)}) %all-gather.8.cloned.1.call-update) | async-done | bytes 10485776 | tf_op jit(solution)/shard_map/all_gather | solution.py:79
  279.8 5.9 %fusion.30 = f32[2048,128]{1,0:T(8,128)S(1)} fusion(bf16[2560,2048]{1,0:T(8,128)(2,1)} %all-gather.8.cloned.1.call-done, bf16[1,2048,128]{2,1,0:T(8,128)(2,1)S(1)} %copy-done), kind=kOutput, calls=%fused_computation.42 | convolution fusion | flops 1073741824 | bytes 9961472 | tf_op jit(solution)/shard_map/dot_general | solution.py:122
  286.1 2.4 fusion.35
  288.8 4.5 stack.2
  293.2 4.9 all-to-all-start.2
  298.2 2.5 fusion.40
  300.7 3.1 fusion.47
  303.9 122.3 %all-to-all-done.2 = bf16[16,2048,128]{1,2,0:T(8,128)(2,1)} async-done(((bf16[16,2048,128]{1,2,0:T(8,128)(2,1)}), bf16[16,2048,128]{1,2,0:T(8,128)(2,1)}, u32[]{:S(2)}, u32[]{:S(2)}) %all-to-all-start.2) | async-done | bytes 8388640 | tf_op jit(solution)/shard_map/all_to_all | solution.py:197
  426.2 6.6 %convolution_convert_fusion = bf16[2048,128]{1,0:T(8,128)(2,1)} fusion(bf16[2048,2048]{0,1:T(8,128)(2,1)} %bitcast.52, bf16[1,2048,128]{2,1,0:T(8,128)(2,1)S(1)} %copy-done.15), kind=kOutput, calls=%fused_computation.45 | convolution fusion | flops 1074003968 | bytes 9437184 | tf_op jit(solution)/shard_map/dot_general | solution.py:122
  432.8 18.8 %all-to-all-start.3 = ((bf16[32,64,128]{2,1,0:T(8,128)(2,1)}), bf16[32,64,128]{2,1,0:T(8,128)(2,1)S(1)}, u32[]{:S(2)}, u32[]{:S(2)}) async-start(bf16[32,64,128]{2,1,0:T(8,128)(2,1)} %bitcast.54), calls=%async_computation.3 | async-start | bytes 1048576 | tf_op jit(solution)/shard_map/all_to_all | solution.py:202
  451.7 33.3 %all-to-all-done.3 = bf16[32,64,128]{2,1,0:T(8,128)(2,1)S(1)} async-done(((bf16[32,64,128]{2,1,0:T(8,128)(2,1)}), bf16[32,64,128]{2,1,0:T(8,128)(2,1)S(1)}, u32[]{:S(2)}, u32[]{:S(2)}) %all-to-all-start.3) | async-done | bytes 524320 | tf_op jit(solution)/shard_map/all_to_all | solution.py:202
  485.1 3.2 gather_fusion.1
  488.3 2.8 fusion.50
  491.1 3.0 fusion.46
  (164 shorter events, 14.2 us)
Async XLA Ops:
  6.5 273.2 %copy-start = (bf16[1,2048,128]{2,1,0:T(8,128)(2,1)S(1)}, bf16[1,2048,128]{2,1,0:T(8,128)(2,1)}, u32[]{:S(2)}) copy-start(bf16[1,2048,128]{2,1,0:T(8,128)(2,1)} %param.30) | copy-start | bytes 1572868
  6.5 71.8 %all-gather.12.cloned.1.call-start = ((), (), s32[]{:S(2)}) async-start(), calls=%async_computation.6 | async-start | bytes 1183744 | tf_op jit(solution)/shard_map/all_gather | solution.py:30
  8.4 1.4 copy-start.3
  8.5 1.4 copy-start.9
  9.2 10.2 %copy-start.5 = (bf16[512,128]{1,0:T(8,128)(2,1)S(1)}, bf16[512,128]{1,0:T(8,128)(2,1)}, u32[]{:S(2)}) copy-start(bf16[512,128]{1,0:T(8,128)(2,1)} %param.19) | copy-start | bytes 393220
  20.0 24.5 %copy-start.6 = (bf16[512,128]{1,0:T(8,128)(2,1)S(1)}, bf16[512,128]{1,0:T(8,128)(2,1)}, u32[]{:S(2)}) copy-start(bf16[512,128]{1,0:T(8,128)(2,1)} %param.22) | copy-start | bytes 393220
  44.4 36.6 %copy-start.10 = (f32[128]{0:T(128)S(1)}, f32[128]{0:T(128)}, u32[]{:S(2)}) copy-start(f32[128]{0:T(128)} %param.24) | copy-start | bytes 1540
  82.8 7.2 %copy-start.7 = (s32[512,2]{0,1:T(2,128)S(1)}, s32[512,2]{0,1:T(2,128)}, u32[]{:S(2)}) copy-start(s32[512,2]{0,1:T(2,128)} %param.28) | copy-start | bytes 12292
  82.8 29.8 %all-to-all-start = ((bf16[16,512,128]{1,2,0:T(8,128)(2,1)}), bf16[16,512,128]{1,2,0:T(8,128)(2,1)S(1)}, u32[]{:S(2)}, u32[]{:S(2)}) async-start(bf16[16,512,128]{1,2,0:T(8,128)(2,1)} %broadcast_in_dim.48), calls=%async_computation | async-start | bytes 4194304 | tf_op jit(solution)/shard_map/all_to_all | solution.py:56
  89.9 22.7 %copy-start.1 = (bf16[2048,128]{1,0:T(8,128)(2,1)S(1)}, bf16[2048,128]{1,0:T(8,128)(2,1)}, u32[]{:S(2)}) copy-start(bf16[2048,128]{1,0:T(8,128)(2,1)} %param.26) | copy-start | bytes 1572868
  89.9 22.7 %copy-start.4 = (bf16[512,128]{1,0:T(8,128)(2,1)S(1)}, bf16[512,128]{1,0:T(8,128)(2,1)}, u32[]{:S(2)}) copy-start(bf16[512,128]{1,0:T(8,128)(2,1)} %param.25) | copy-start | bytes 393220
  89.9 189.9 %all-gather.8.cloned.1.call-start = ((), (), s32[]{:S(2)}) async-start(), calls=%async_computation.4 | async-start | bytes 11141120 | tf_op jit(solution)/shard_map/all_gather | solution.py:79
  190.6 95.1 %copy-start.12 = (bf16[1,2048,128]{2,1,0:T(8,128)(2,1)S(1)}, bf16[1,2048,128]{2,1,0:T(8,128)(2,1)}, u32[]{:S(2)}) copy-start(bf16[1,2048,128]{2,1,0:T(8,128)(2,1)} %param.31) | copy-start | bytes 1572868
  279.8 6.4 %copy-start.11 = (bf16[2560,2048]{1,0:T(8,128)(2,1)S(1)}, bf16[2560,2048]{1,0:T(8,128)(2,1)}, u32[]{:S(2)}) copy-start(bf16[2560,2048]{1,0:T(8,128)(2,1)} %all-gather.8.cloned.1.call-done) | copy-start | bytes 31457284
  293.2 5.0 copy-start.13
  293.2 133.0 %all-to-all-start.2 = ((bf16[16,2048,128]{1,2,0:T(8,128)(2,1)}), bf16[16,2048,128]{1,2,0:T(8,128)(2,1)}, u32[]{:S(2)}, u32[]{:S(2)}) async-start(bf16[16,2048,128]{1,2,0:T(8,128)(2,1)} %stack.2), calls=%async_computation.2 | async-start | bytes 16777216 | tf_op jit(solution)/shard_map/all_to_all | solution.py:197
  298.2 2.5 copy-start.14
  298.2 192.9 %all-gather.10.cloned.1.call-start = ((), (), s32[]{:S(2)}) async-start(), calls=%async_computation.5 | async-start | bytes 2228224 | tf_op jit(solution)/shard_map/all_gather | solution.py:195
  300.7 125.5 %copy-start.15 = (bf16[1,2048,128]{2,1,0:T(8,128)(2,1)S(1)}, bf16[1,2048,128]{2,1,0:T(8,128)(2,1)}, u32[]{:S(2)}) copy-start(bf16[1,2048,128]{2,1,0:T(8,128)(2,1)} %param.32) | copy-start | bytes 1572868
  426.2 25.4 %copy-start.8 = (f32[512,2]{0,1:T(2,128)S(1)}, f32[512,2]{0,1:T(2,128)}, u32[]{:S(2)}) copy-start(f32[512,2]{0,1:T(2,128)} %param.29) | copy-start | bytes 12292
  432.8 58.3 %copy-start.2 = (bf16[2048,128]{1,0:T(8,128)(2,1)S(1)}, bf16[2048,128]{1,0:T(8,128)(2,1)}, u32[]{:S(2)}) copy-start(bf16[2048,128]{1,0:T(8,128)(2,1)} %param.35) | copy-start | bytes 1572868
  432.8 52.3 %all-to-all-start.3 = ((bf16[32,64,128]{2,1,0:T(8,128)(2,1)}), bf16[32,64,128]{2,1,0:T(8,128)(2,1)S(1)}, u32[]{:S(2)}, u32[]{:S(2)}) async-start(bf16[32,64,128]{2,1,0:T(8,128)(2,1)} %bitcast.54), calls=%async_computation.3 | async-start | bytes 1048576 | tf_op jit(solution)/shard_map/all_to_all | solution.py:202
Sparse Core Ops, SparseCore 0:
  19.5 58.8 all-gather.11
  190.7 89.0 all-gather.7
  304.0 125.4 all-gather.9
